TPU v7x, 32 devices: a whole 2x2x4 slice. The times are simulated.
32 devices in a mesh: ep: 8 (over z, y), tp: 4 (over x, core).
Axes of the slice: x: 2, y: 2, z: 4, core: 2. Of those that a mesh axis runs over, the one named last changes fastest.
Arguments:
- tokens: bfloat16 [128, 2048], P('ep', 'tp'), may hold values from -40 to 40
- kv_cache: bfloat16 [128, 1024, 512], P('ep', None, 'tp'), may hold values from -1000 to 1000
- cum_gate: float32 [128, 16, 1024], P('ep', 'tp'), may hold values from -400 to 0, as said below
- lengths: int32 [128], P('ep'), may hold values from 256 to 1024
- w_query: bfloat16 [2048, 1024], P(None, 'tp'), may hold values from -0.125 to 0.125
- w_key: bfloat16 [2048, 256], P(None, 'tp'), may hold values from -0.125 to 0.125
- w_value: bfloat16 [2048, 256], P(None, 'tp'), may hold values from -0.125 to 0.125
- w_forget: bfloat16 [2048, 16], P(None, 'tp'), may hold values from -0.5 to 0.5
- forget_bias: float32 [16], P('tp'), may hold values from -2.5 to 1.5
- w_out: bfloat16 [1024, 2048], P('tp'), may hold values from -0.1875 to 0.1875
- attn_gain: bfloat16 [2048], replicated, may hold values from 0.099609375 to 1.8984375
- ffn_gain: bfloat16 [2048], replicated, may hold values from 0.099609375 to 1.8984375
- mix_gate: bfloat16 [2048], replicated, may hold values from -0.125 to 0.125
- expert_gate: bfloat16 [8, 2048, 1024], P('ep', None, 'tp'), may hold values from -0.125 to 0.125
- expert_up: bfloat16 [8, 2048, 1024], P('ep', None, 'tp'), may hold values from -0.125 to 0.125
- expert_down: bfloat16 [8, 1024, 2048], P('ep', 'tp'), may hold values from -0.1875 to 0.1875
- chosen: int32 [128, 2], P('ep'), may hold values from 0 to 7, as said below
- route_weight: float32 [128, 2], P('ep'), may hold values from 0.5 to 1.5
- dense_gate: bfloat16 [2048, 1024], P(None, 'tp'), may hold values from -0.125 to 0.125
- dense_up: bfloat16 [2048, 1024], P(None, 'tp'), may hold values from -0.125 to 0.125
- dense_down: bfloat16 [1024, 2048], P('tp'), may hold values from -0.1875 to 0.1875
Outputs:
- mixed: bfloat16 [128, 2048], P('ep', 'tp')
Inputs may be any that keep to these rules, and one draw needn't show every extreme that they name: `cum_gate`: along positions each row never rises: entry p is the sum of the log forget gates of positions 0 to p of that sequence and head. `chosen`: each row names two different experts of one group of 8 consecutive expert numbers. The rows of one device name any one expert at most 8 times, and some expert exactly 8 times.
All inputs are finite; a program needn't handle non-finite values.
Results may differ from a plain program's by a relative error of at most 0.014.
Values may be sent and summed in bfloat16 or wider, within the bound.
A program may use at most 64 MiB of HBM per device.

v0:
```python
import jax
import jax.numpy as jnp
from jax import lax
from jax.sharding import PartitionSpec as P

HD = 64
TOP = 2
epsilon = 1e-06


def norm_rows(values, scales):
    widened = values.astype(jnp.float32)
    square = jnp.mean(widened * widened, axis=-1, keepdims=True)
    return (widened * lax.rsqrt(square + epsilon) * scales.astype(jnp.float32)).astype(jnp.bfloat16)


def attend(h_one, kv_cache, cum_gate, lengths, w_query, w_key, w_value, w_forget, forget_bias):
    tok_count = h_one.shape[0]
    cache_len = kv_cache.shape[1]
    kv_local = w_key.shape[1] // HD
    q_local = w_query.shape[1] // HD
    group_size = q_local // kv_local
    score_scale = HD ** (-0.5)
    queries = jnp.dot(h_one, w_query, preferred_element_type=jnp.float32).astype(jnp.bfloat16)
    queries = queries.reshape(tok_count, kv_local, group_size, HD)
    key_new = jnp.dot(h_one, w_key, preferred_element_type=jnp.float32).astype(jnp.bfloat16)
    key_new = key_new.reshape(tok_count, kv_local, HD)
    value_new = jnp.dot(h_one, w_value, preferred_element_type=jnp.float32).astype(jnp.bfloat16)
    value_new = value_new.reshape(tok_count, kv_local, HD)
    forget_now = jax.nn.log_sigmoid(
        jnp.dot(h_one, w_forget, preferred_element_type=jnp.float32) + forget_bias
    )
    forget_now = forget_now.reshape(tok_count, kv_local, group_size)
    stacked = kv_cache.reshape(tok_count, cache_len, kv_local, 2, HD)
    past_keys = stacked[:, :, :, 0, :]
    past_values = stacked[:, :, :, 1, :]
    scores = (
        jnp.einsum("sjgd,scjd->sjgc", queries, past_keys, preferred_element_type=jnp.float32)
        * score_scale
    )
    cumulative = cum_gate.reshape(tok_count, kv_local, group_size, cache_len)
    position_rows = jnp.arange(cache_len, dtype=jnp.int32)
    at_last = (position_rows[None, :] == (lengths - 1)[:, None]).astype(jnp.float32)
    latest = jnp.sum(cumulative * at_last[:, None, None, :], axis=-1, keepdims=True)
    scores = scores + latest - cumulative + forget_now[:, :, :, None]
    inside = position_rows[None, :] < lengths[:, None]
    scores = jnp.where(inside[:, None, None, :], scores, -jnp.inf)
    own_score = (
        jnp.einsum("sjgd,sjd->sjg", queries, key_new, preferred_element_type=jnp.float32)
        * score_scale
    )
    highest = jnp.maximum(jnp.max(scores, axis=-1), own_score)
    weights = jnp.exp(scores - highest[:, :, :, None])
    own_weight = jnp.exp(own_score - highest)
    denominator = jnp.sum(weights, axis=-1) + own_weight
    weights = (weights / denominator[:, :, :, None]).astype(jnp.bfloat16)
    own_weight = (own_weight / denominator).astype(jnp.bfloat16)
    blended = jnp.einsum(
        "sjgc,scjd->sjgd", weights, past_values, preferred_element_type=jnp.float32
    )
    blended = (
        blended
        + own_weight.astype(jnp.float32)[:, :, :, None]
        * value_new.astype(jnp.float32)[:, :, None, :]
    )
    return blended.astype(jnp.bfloat16).reshape(tok_count, q_local * HD)


def local(
    tokens,
    kv_cache,
    cum_gate,
    lengths,
    w_query,
    w_key,
    w_value,
    w_forget,
    forget_bias,
    w_out,
    attn_gain,
    ffn_gain,
    mix_gate,
    expert_gate,
    expert_up,
    expert_down,
    chosen,
    route_weight,
    dense_gate,
    dense_up,
    dense_down,
):
    tok_count = tokens.shape[0]
    slice_width = tokens.shape[1]
    ep_count = lax.axis_size("ep")
    gathered = lax.all_gather(tokens, "tp", axis=1, tiled=True)
    model_width = gathered.shape[1]
    h_one = norm_rows(gathered, attn_gain)
    head_out = attend(
        h_one, kv_cache, cum_gate, lengths, w_query, w_key, w_value, w_forget, forget_bias
    )
    partial_value = jnp.dot(head_out, w_out, preferred_element_type=jnp.float32)
    tp_offset = lax.axis_index("tp") * slice_width
    attention = lax.psum(partial_value.astype(jnp.bfloat16), "tp").astype(jnp.float32)
    residual_full = (gathered.astype(jnp.float32) + attention).astype(jnp.bfloat16)
    h_two = norm_rows(residual_full, ffn_gain)
    residual = lax.dynamic_slice_in_dim(residual_full, tp_offset, slice_width, 1)
    capacity = max(2, (4 * tok_count + ep_count - 1) // ep_count)
    routes = chosen.reshape(-1)
    expert_ids = jnp.arange(ep_count, dtype=jnp.int32)
    one_hot = (routes[:, None] == expert_ids[None, :]).astype(jnp.int32)
    rank_of = jnp.sum((jnp.cumsum(one_hot, axis=0) - one_hot) * one_hot, axis=1)
    slot_of = routes * capacity + rank_of
    slot_ids = jnp.arange(ep_count * capacity, dtype=jnp.int32)
    chooser = (slot_ids[:, None] == slot_of[None, :]).astype(jnp.bfloat16)
    per_token = jnp.sum(chooser.reshape(ep_count * capacity, tok_count, TOP), axis=2)
    outgoing = jnp.dot(per_token, h_two, preferred_element_type=jnp.float32).astype(jnp.bfloat16)
    outgoing = outgoing.reshape(ep_count, capacity, model_width)
    received = lax.all_to_all(outgoing, "ep", split_axis=0, concat_axis=0, tiled=True)
    flat_rows = received.reshape(-1, model_width)
    gate_pre = jnp.dot(flat_rows, expert_gate[0], preferred_element_type=jnp.float32)
    up_pre = jnp.dot(flat_rows, expert_up[0], preferred_element_type=jnp.float32)
    hidden = (jax.nn.silu(gate_pre) * up_pre).astype(jnp.bfloat16)
    part_out = jnp.dot(hidden, expert_down[0], preferred_element_type=jnp.float32)
    summed = lax.psum_scatter(part_out.astype(jnp.bfloat16), "tp", scatter_dimension=1, tiled=True)
    shares = summed.reshape(received.shape[0], received.shape[1], -1)
    returned = lax.all_to_all(shares, "ep", split_axis=0, concat_axis=0, tiled=True)
    returned = returned.reshape(ep_count * capacity, slice_width)
    picked = jnp.dot(chooser.T, returned, preferred_element_type=jnp.float32)
    routed_sum = jnp.sum(
        picked.reshape(tok_count, TOP, slice_width) * route_weight[:, :, None], axis=1
    )
    dense_pre = jnp.dot(h_two, dense_gate, preferred_element_type=jnp.float32)
    dense_lift = jnp.dot(h_two, dense_up, preferred_element_type=jnp.float32)
    dense_act = (jax.nn.silu(dense_pre) * dense_lift).astype(jnp.bfloat16)
    dense_part = jnp.dot(dense_act, dense_down, preferred_element_type=jnp.float32)
    dense_out = lax.psum_scatter(
        dense_part.astype(jnp.bfloat16), "tp", scatter_dimension=1, tiled=True
    ).astype(jnp.float32)
    blend_gate = jax.nn.sigmoid(jnp.dot(h_two, mix_gate, preferred_element_type=jnp.float32))
    return (residual.astype(jnp.float32) + routed_sum + blend_gate[:, None] * dense_out).astype(
        jnp.bfloat16
    )


def solution(mesh):
    in_specs = (
        P("ep", "tp"),
        P("ep", None, "tp"),
        P("ep", "tp", None),
        P("ep"),
        P(None, "tp"),
        P(None, "tp"),
        P(None, "tp"),
        P(None, "tp"),
        P("tp"),
        P("tp", None),
        P(),
        P(),
        P(),
        P("ep", None, "tp"),
        P("ep", None, "tp"),
        P("ep", "tp", None),
        P("ep", None),
        P("ep", None),
        P(None, "tp"),
        P(None, "tp"),
        P("tp", None),
    )
    out_specs = P("ep", "tp")
    return jax.shard_map(local, mesh=mesh, in_specs=in_specs, out_specs=out_specs, check_vma=False)
```

profile of v0, /device:TPU:0, one launch (start us, length us, event | category | flops | bytes accessed | tf_op | source)
XLA Modules:
  0.0 130.5 jit_solution(5122951195548866926)
XLA Ops:
  6.5 6.6 %all_gather.3 = bf16[16,2048]{1,0:T(8,128)(2,1)S(1)} all-gather(bf16[16,512]{1,0:T(8,128)(2,1)} %param.21), channel_id=1, replica_groups=mesh['ep'=8,'tp'=4] {'tp'}, dimensions={1}, use_global_device_ids=true | all-gather | bytes 81920 | tf_op jit(solution)/shard_map/all_gather | solution.py:95
  13.3 0.7 convert_element_type.98
  13.9 1.5 %convolution_convert_fusion.4 = bf16[16,256]{1,0:T(8,128)(2,1)S(1)} fusion(bf16[2048,256]{1,0:T(8,128)(2,1)} %param.25, bf16[16,2048]{1,0:T(8,128)(2,1)S(1)} %all_gather.3, f32[2048]{0:T(1024)S(1)} %convert_element_type.98, f32[16]{0:T(128)S(1)} %add_rsqrt_fusion.1), kind=kOutput, calls=%fused_computation.23 | convolution fusion | flops 16912384 | bytes 1130560 | tf_op jit(solution)/shard_map/dot_general | solution.py:24
  15.6 6.5 %copy.43 = bf16[16,1024,128]{1,2,0:T(8,128)(2,1)} copy(bf16[16,1024,128]{2,1,0:T(8,128)(2,1)} %param.22) | data formatting | bytes 8388608 | tf_op args[1]
  22.7 2.2 %fusion.8 = f32[16,4,1024]{2,1,0:T(4,128)S(1)} fusion(bf16[16,4,64]{2,1,0:T(4,128)(2,1)S(1)} %reshape.204, bf16[16,1024,1,2,64]{1,4,3,0,2:T(8,128)(2,1)} %bitcast.68), kind=kOutput, calls=%fused_computation.14 | convolution fusion | flops 8454144 | bytes 2367488 | tf_op jit(solution)/shard_map/sjgd,scjd->sjgc/dot_general | solution.py:38
  25.9 0.7 fusion.12
  26.7 2.2 %convolution_convert_fusion.3 = bf16[16,2048]{1,0:T(8,128)(2,1)} fusion(bf16[16,256]{1,0:T(8,128)(2,1)S(1)} %reshape.208, bf16[256,2048]{1,0:T(8,128)(2,1)} %param.30), kind=kOutput, calls=%fused_computation.5 | convolution fusion | flops 16809984 | bytes 1122304 | tf_op jit(solution)/shard_map/dot_general | solution.py:101
  29.8 32.6 %all-reduce.2.cloned.1.call-done = bf16[16,2048]{1,0:T(8,128)(2,1)} async-done(((bf16[16,2048]{1,0:T(8,128)(2,1)}), bf16[16,2048]{1,0:T(8,128)(2,1)}) %all-reduce.2.cloned.1.call-update) | async-done | bytes 65552 | tf_op jit(solution)/shard_map/psum | solution.py:103
  62.4 1.0 fusion.31
  63.4 1.0 fusion.1
  64.3 5.5 %all-to-all-start = ((bf16[8,8,2048]{2,1,0:T(8,128)(2,1)}), bf16[8,8,2048]{2,1,0:T(8,128)(2,1)S(1)}, u32[]{:S(2)}, u32[]{:S(2)}) async-start(bf16[8,8,2048]{2,1,0:T(8,128)(2,1)} %fusion.1), calls=%async_computation | async-start | bytes 524288 | tf_op jit(solution)/shard_map/all_to_all | solution.py:118
  69.9 0.6 reshape.217
  70.6 7.5 %all-to-all-done = bf16[8,8,2048]{2,1,0:T(8,128)(2,1)S(1)} async-done(((bf16[8,8,2048]{2,1,0:T(8,128)(2,1)}), bf16[8,8,2048]{2,1,0:T(8,128)(2,1)S(1)}, u32[]{:S(2)}, u32[]{:S(2)}) %all-to-all-start) | async-done | bytes 262176 | tf_op jit(solution)/shard_map/all_to_all | solution.py:118
  78.1 1.5 %fusion.24 = f32[64,256]{1,0:T(8,128)S(1)} fusion(bf16[1,2048,256]{2,1,0:T(8,128)(2,1)} %param.34, bf16[8,8,2048]{2,1,0:T(8,128)(2,1)S(1)} %all-to-all-done), kind=kOutput, calls=%fused_computation.37 | convolution fusion | flops 67108864 | bytes 1376256 | tf_op jit(solution)/shard_map/dot_general | solution.py:120
  79.6 2.7 %convolution_convert_fusion = bf16[64,2048]{1,0:T(8,128)(2,1)} fusion(bf16[1,256,2048]{2,1,0:T(8,128)(2,1)S(1)} %copy-done, bf16[1,2048,256]{2,1,0:T(8,128)(2,1)} %param.35, bf16[8,8,2048]{2,1,0:T(8,128)(2,1)S(1)} %all-to-all-done, f32[64,256]{1,0:T(8,128)S(1)} %fusion.24), kind=kOutput, calls=%fused_computation.1 | convolution fusion | flops 134447104 | bytes 2686976 | tf_op jit(solution)/shard_map/dot_general | solution.py:123
  82.4 1.5 %fusion.72 = f32[16,256]{1,0:T(8,128)S(1)} fusion(bf16[2048,256]{1,0:T(8,128)(2,1)} %param.39, bf16[16,2048]{1,0:T(8,128)(2,1)S(1)} %get-tuple-element.6, f32[2048]{0:T(1024)S(1)} %convert_element_type.116, f32[16]{0:T(128)} %copy-done.4), kind=kOutput, calls=%fused_computation.102 | convolution fusion | flops 16908288 | bytes 1138752 | tf_op jit(solution)/shard_map/dot_general | solution.py:132
  83.9 2.0 %convolution_convert_fusion.2 = bf16[16,2048]{1,0:T(8,128)(2,1)} fusion(bf16[256,2048]{1,0:T(8,128)(2,1)S(1)} %copy-done.2, bf16[2048,256]{1,0:T(8,128)(2,1)S(1)} %copy-done.3, f32[16,256]{1,0:T(8,128)S(1)} %fusion.72, bf16[16,2048]{1,0:T(8,128)(2,1)S(1)} %get-tuple-element.6, f32[2048]{0:T(1024)S(1)} %convert_element_type.116, f32[16]{0:T(128)} %copy-done.4), kind=kOutput, calls=%fused_computation.4 | convolution fusion | flops 33742848 | bytes 2252864 | tf_op jit(solution)/shard_map/dot_general | solution.py:135
  86.0 14.6 %reduce-scatter.3.cloned.1.call-done = bf16[64,512]{1,0:T(8,128)(2,1)} async-done(((bf16[64,2048]{1,0:T(8,128)(2,1)}), bf16[64,512]{1,0:T(8,128)(2,1)}) %reduce-scatter.3.cloned.1.call-update) | async-done | bytes 65552 | tf_op jit(solution)/shard_map/reduce_scatter | solution.py:124
  100.5 5.5 %all-to-all-start.1 = ((bf16[8,8,512]{2,1,0:T(8,128)(2,1)}), bf16[8,8,512]{2,1,0:T(8,128)(2,1)S(1)}, u32[]{:S(2)}, u32[]{:S(2)}) async-start(bf16[8,8,512]{2,1,0:T(8,128)(2,1)} %bitcast.70), calls=%async_computation.2 | async-start | bytes 131072 | tf_op jit(solution)/shard_map/all_to_all | solution.py:126
  106.0 0.9 fusion.20
  106.9 6.0 %all-to-all-done.1 = bf16[8,8,512]{2,1,0:T(8,128)(2,1)S(1)} async-done(((bf16[8,8,512]{2,1,0:T(8,128)(2,1)}), bf16[8,8,512]{2,1,0:T(8,128)(2,1)S(1)}, u32[]{:S(2)}, u32[]{:S(2)}) %all-to-all-start.1) | async-done | bytes 65568 | tf_op jit(solution)/shard_map/all_to_all | solution.py:126
  112.9 0.8 fusion.10
  113.8 8.8 %reduce-scatter.5.cloned.1.call-done = bf16[16,512]{1,0:T(8,128)(2,1)} async-done(((bf16[16,2048]{1,0:T(8,128)(2,1)}), bf16[16,512]{1,0:T(8,128)(2,1)}) %reduce-scatter.5.cloned.1.call-update) | async-done | bytes 16400 | tf_op jit(solution)/shard_map/reduce_scatter | solution.py:136
  122.5 1.4 %add_convert_fusion = bf16[16,512]{1,0:T(8,128)(2,1)} fusion(bf16[16,512]{1,0:T(8,128)(2,1)} %reduce-scatter.5.cloned.1.call-done, f32[16,512]{1,0:T(8,128)S(1)} %fusion.10, f32[16]{0:T(128)S(1)} %fusion.20, bf16[16,2048]{1,0:T(8,128)(2,1)S(1)} %get-tuple-element.6, s32[]{:T(128)S(6)} %select_n.15), kind=kLoop, calls=%fused_computation.70 | loop fusion | flops 49152 | bytes 81988 | tf_op jit(solution)/shard_map/convert_element_type | solution.py:140
  (63 shorter events, 2.9 us)
Async XLA Ops:
  6.5 73.1 %copy-start = (bf16[1,256,2048]{2,1,0:T(8,128)(2,1)S(1)}, bf16[1,256,2048]{2,1,0:T(8,128)(2,1)}, u32[]{:S(2)}) copy-start(bf16[1,256,2048]{2,1,0:T(8,128)(2,1)} %param.36) | copy-start | bytes 3145732
  6.5 55.8 %all-reduce.2.cloned.1.call-start = ((), (), s32[]{:S(2)}) async-start(), calls=%async_computation.4 | async-start | bytes 131072 | tf_op jit(solution)/shard_map/psum | solution.py:103
  15.5 6.5 %copy-start.12 = (bf16[2048,4]{0,1:T(4,128)(2,1)S(1)}, bf16[2048,4]{0,1:T(4,128)(2,1)}, u32[]{:S(2)}) copy-start(bf16[2048,4]{0,1:T(4,128)(2,1)} %param.28) | copy-start | bytes 49156
  15.6 6.5 %copy-start.13 = (f32[4]{0:T(128)S(1)}, f32[4]{0:T(128)}, u32[]{:S(2)}) copy-start(f32[4]{0:T(128)} %param.29) | copy-start | bytes 52
  15.6 6.8 %copy-start.8 = (s32[16]{0:T(128)S(1)}, s32[16]{0:T(128)}, u32[]{:S(2)}) copy-start(s32[16]{0:T(128)} %param.24) | copy-start | bytes 196
  15.6 6.9 %copy-start.9 = (bf16[2048,64]{0,1:T(8,128)(2,1)S(1)}, bf16[2048,64]{0,1:T(8,128)(2,1)}, u32[]{:S(2)}) copy-start(bf16[2048,64]{0,1:T(8,128)(2,1)} %param.26) | copy-start | bytes 786436
  15.6 9.5 %copy-start.10 = (f32[16,4,1024]{2,1,0:T(4,128)S(1)}, f32[16,4,1024]{2,1,0:T(4,128)}, u32[]{:S(2)}) copy-start(f32[16,4,1024]{2,1,0:T(4,128)} %param.23) | copy-start | bytes 786436
  22.1 3.6 %copy-start.11 = (bf16[2048,64]{0,1:T(8,128)(2,1)S(1)}, bf16[2048,64]{0,1:T(8,128)(2,1)}, u32[]{:S(2)}) copy-start(bf16[2048,64]{0,1:T(8,128)(2,1)} %param.27) | copy-start | bytes 786436
  22.4 3.5 %copy-start.1 = (bf16[16,1024,128]{1,2,0:T(8,128)(2,1)S(1)}, bf16[16,1024,128]{1,2,0:T(8,128)(2,1)}, u32[]{:S(2)}) copy-start(bf16[16,1024,128]{1,2,0:T(8,128)(2,1)} %copy.43) | copy-start | bytes 12582916
  24.9 4.1 %copy-start.7 = (s32[16,2]{0,1:T(2,128)S(1)}, s32[16,2]{0,1:T(2,128)}, u32[]{:S(2)}) copy-start(s32[16,2]{0,1:T(2,128)} %param.37) | copy-start | bytes 388
  24.9 4.8 %copy-start.5 = (bf16[2048]{0:T(1024)(128)(2,1)S(1)}, bf16[2048]{0:T(1024)(128)(2,1)}, u32[]{:S(2)}) copy-start(bf16[2048]{0:T(1024)(128)(2,1)} %param.32) | copy-start | bytes 12292
  25.1 44.8 %copy-start.6 = (bf16[2048]{0:T(1024)(128)(2,1)S(1)}, bf16[2048]{0:T(1024)(128)(2,1)}, u32[]{:S(2)}) copy-start(bf16[2048]{0:T(1024)(128)(2,1)} %param.33) | copy-start | bytes 12292
  26.6 57.3 %copy-start.2 = (bf16[256,2048]{1,0:T(8,128)(2,1)S(1)}, bf16[256,2048]{1,0:T(8,128)(2,1)}, u32[]{:S(2)}) copy-start(bf16[256,2048]{1,0:T(8,128)(2,1)} %param.41) | copy-start | bytes 3145732
  26.6 57.3 %copy-start.3 = (bf16[2048,256]{1,0:T(8,128)(2,1)S(1)}, bf16[2048,256]{1,0:T(8,128)(2,1)}, u32[]{:S(2)}) copy-start(bf16[2048,256]{1,0:T(8,128)(2,1)} %param.40) | copy-start | bytes 3145732
  63.4 1.0 copy-start.4
  64.3 13.7 %all-to-all-start = ((bf16[8,8,2048]{2,1,0:T(8,128)(2,1)}), bf16[8,8,2048]{2,1,0:T(8,128)(2,1)S(1)}, u32[]{:S(2)}, u32[]{:S(2)}) async-start(bf16[8,8,2048]{2,1,0:T(8,128)(2,1)} %fusion.1), calls=%async_computation | async-start | bytes 524288 | tf_op jit(solution)/shard_map/all_to_all | solution.py:118
  69.9 30.7 %reduce-scatter.3.cloned.1.call-start = ((), (), s32[]{:S(2)}) async-start(), calls=%async_computation.5 | async-start | bytes 327680 | tf_op jit(solution)/shard_map/reduce_scatter | solution.py:124
  82.4 40.2 %reduce-scatter.5.cloned.1.call-start = ((), (), s32[]{:S(2)}) async-start(), calls=%async_computation.6 | async-start | bytes 81920 | tf_op jit(solution)/shard_map/reduce_scatter | solution.py:136
  100.5 12.4 %all-to-all-start.1 = ((bf16[8,8,512]{2,1,0:T(8,128)(2,1)}), bf16[8,8,512]{2,1,0:T(8,128)(2,1)S(1)}, u32[]{:S(2)}, u32[]{:S(2)}) async-start(bf16[8,8,512]{2,1,0:T(8,128)(2,1)} %bitcast.70), calls=%async_computation.2 | async-start | bytes 131072 | tf_op jit(solution)/shard_map/all_to_all | solution.py:126
Sparse Core Ops, SparseCore 0:
  29.1 33.2 all-reduce.1
  82.5 18.0 reduce-scatter.2
  103.0 19.5 reduce-scatter.4
where the time goes:
time: 131 us; the launch traced here: 130 us
  waiting for transfers between devices  69.4 us (53%)
  matrix products  17.9 us (14%)
  between operations  13.3 us (10%)
  starting transfers between devices  11.1 us (8%)
  local copies, waits for them, and re-layouts  7.77 us (6%)
  blocking collectives  6.57 us (5%)
  other arithmetic  4.38 us (3%)
    psum x1, waiting for transfers between devices, local(): lax.psum(partial_value.astype(jnp.bfloat16), 'tp').astype(jnp.float32)  32.6 us
    reduce_scatter x1, waiting for transfers between devices, local(): lax.psum_scatter(part_out.astype(jnp.bfloat16), 'tp', scatter_dimension=1...  14.6 us
    reduce_scatter x1, waiting for transfers between devices, local(): lax.psum_scatter(dense_part.astype(jnp.bfloat16), 'tp', scatter_dimension...  8.77 us
    all_to_all x1, waiting for transfers between devices, local(): lax.all_to_all(outgoing, 'ep', split_axis=0, concat_axis=0, tiled=True)  7.45 us
    unnamed x31, local copies, waits for them, and re-layouts  7.22 us
    all_gather x1, blocking collectives, local(): gathered = lax.all_gather(tokens, 'tp', axis=1, tiled=True)  6.57 us
    all_to_all x1, waiting for transfers between devices, local(): lax.all_to_all(shares, 'ep', split_axis=0, concat_axis=0, tiled=True)  6 us
    all_to_all x1, starting transfers between devices, local(): lax.all_to_all(outgoing, 'ep', split_axis=0, concat_axis=0, tiled=True)  5.52 us
  transfers between devices with their start and end apart: 5, of which 5 were waited for; matrix products, arithmetic and copies ran while one was open for 5% of the time, Pallas kernels for 0%

commit v1 on v0

--- a/solution.py
+++ b/solution.py
@@ -6,6 +6,12 @@
 HD = 64
 TOP = 2
 epsilon = 1e-06
+
+
+def summed_here(x, name):
+    parts = lax.all_gather(x, name, axis=0, tiled=False)
+    summed = parts.sum(axis=0)
+    return summed
 
 
 def norm_rows(values, scales):
@@ -100,7 +106,7 @@
     )
     partial_value = jnp.dot(head_out, w_out, preferred_element_type=jnp.float32)
     tp_offset = lax.axis_index("tp") * slice_width
-    attention = lax.psum(partial_value.astype(jnp.bfloat16), "tp").astype(jnp.float32)
+    attention = summed_here(partial_value.astype(jnp.bfloat16), "tp").astype(jnp.float32)
     residual_full = (gathered.astype(jnp.float32) + attention).astype(jnp.bfloat16)
     h_two = norm_rows(residual_full, ffn_gain)
     residual = lax.dynamic_slice_in_dim(residual_full, tp_offset, slice_width, 1)

time: 131 us -> 108 us (0.82)
  waiting for transfers between devices: 69.4 us -> 30.2 us
  blocking collectives: 6.57 us -> 27.9 us
  starting transfers between devices: 11.1 us -> 5.56 us
  matrix products: 17.9 us -> 15.3 us
  other arithmetic: 4.38 us -> 6.38 us
    psum x1 -> x0, waiting for transfers between devices: 32.6 us -> none  [local(): lax.psum(partial_value.astype(jnp.bfloat16), 'tp').astype(jnp.float32)]
    all_to_all x0 -> x1, blocking collectives: none -> 15.2 us  [local(): lax.all_to_all(outgoing, 'ep', split_axis=0, concat_axis=0, tiled=True)]
    all_to_all x1 -> x0, waiting for transfers between devices: 7.45 us -> none  [local(): lax.all_to_all(outgoing, 'ep', split_axis=0, concat_axis=0, tiled=True)]
    all_gather x0 -> x1, blocking collectives: none -> 6.21 us  [summed_here(): parts = lax.all_gather(x, name, axis=0, tiled=False)]
    all_to_all x1 -> x0, starting transfers between devices: 5.52 us -> none  [local(): lax.all_to_all(outgoing, 'ep', split_axis=0, concat_axis=0, tiled=True)]
    add x2, other arithmetic: 0.01 us -> 1.36 us  [local(): slot_of = routes * capacity + rank_of]
    unnamed x31 -> x27, local copies, waits for them, and re-layouts: 7.22 us -> 7.98 us
  transfers between devices with their start and end apart: 5 -> 3, of which waited for: 5 -> 3; matrix products, arithmetic and copies ran while one was open for 5% -> 5% of each run, Pallas kernels for 0% -> 0%
where the time goes in v1:
time: 108 us; the launch traced here: 107 us
  waiting for transfers between devices  30.2 us (28%)
  blocking collectives  27.9 us (26%)
  matrix products  15.3 us (14%)
  between operations  13.6 us (13%)
  local copies, waits for them, and re-layouts  8.52 us (8%)
  other arithmetic  6.38 us (6%)
  starting transfers between devices  5.56 us (5%)
    all_to_all x1, blocking collectives, local(): lax.all_to_all(outgoing, 'ep', split_axis=0, concat_axis=0, tiled=True)  15.2 us
    reduce_scatter x1, waiting for transfers between devices, local(): lax.psum_scatter(part_out.astype(jnp.bfloat16), 'tp', scatter_dimension=1...  14.6 us
    reduce_scatter x1, waiting for transfers between devices, local(): lax.psum_scatter(dense_part.astype(jnp.bfloat16), 'tp', scatter_dimension...  8.75 us
    unnamed x27, local copies, waits for them, and re-layouts  7.98 us
    all_to_all x1, waiting for transfers between devices, local(): lax.all_to_all(shares, 'ep', split_axis=0, concat_axis=0, tiled=True)  6.81 us
    all_gather x1, blocking collectives, local(): gathered = lax.all_gather(tokens, 'tp', axis=1, tiled=True)  6.57 us
    all_gather x1, blocking collectives, summed_here(): parts = lax.all_gather(x, name, axis=0, tiled=False)  6.21 us
    all_to_all x1, starting transfers between devices, local(): lax.all_to_all(shares, 'ep', split_axis=0, concat_axis=0, tiled=True)  5.52 us
  transfers between devices with their start and end apart: 3, of which 3 were waited for; matrix products, arithmetic and copies ran while one was open for 5% of the time, Pallas kernels for 0%

profile of v1, /device:TPU:0, one launch (start us, length us, event | category | flops | bytes accessed | tf_op | source)
XLA Modules:
  0.0 107.5 jit_solution(16837346550059615981)
XLA Ops:
  6.5 6.6 %all_gather.9 = bf16[16,2048]{1,0:T(8,128)(2,1)S(1)} all-gather(bf16[16,512]{1,0:T(8,128)(2,1)} %param.21), channel_id=1, replica_groups=mesh['ep'=8,'tp'=4] {'tp'}, dimensions={1}, use_global_device_ids=true | all-gather | bytes 81920 | tf_op jit(solution)/shard_map/all_gather | solution.py:101
  13.3 0.7 convert_element_type.100
  13.9 1.5 %convolution_convert_fusion.4 = bf16[16,256]{1,0:T(8,128)(2,1)S(1)} fusion(bf16[2048,256]{1,0:T(8,128)(2,1)} %param.25, bf16[16,2048]{1,0:T(8,128)(2,1)S(1)} %all_gather.9, f32[2048]{0:T(1024)S(1)} %convert_element_type.100, f32[16]{0:T(128)S(1)} %add_rsqrt_fusion.1), kind=kOutput, calls=%fused_computation.23 | convolution fusion | flops 16912384 | bytes 1130560 | tf_op jit(solution)/shard_map/dot_general | solution.py:30
  15.6 6.5 %copy.43 = bf16[16,1024,128]{1,2,0:T(8,128)(2,1)} copy(bf16[16,1024,128]{2,1,0:T(8,128)(2,1)} %param.22) | data formatting | bytes 8388608 | tf_op args[1]
  22.7 2.2 %fusion.8 = f32[16,4,1024]{2,1,0:T(4,128)S(1)} fusion(bf16[16,4,64]{2,1,0:T(4,128)(2,1)S(1)} %reshape.204, bf16[16,1024,1,2,64]{1,4,3,0,2:T(8,128)(2,1)} %bitcast.69), kind=kOutput, calls=%fused_computation.14 | convolution fusion | flops 8454144 | bytes 2367488 | tf_op jit(solution)/shard_map/sjgd,scjd->sjgc/dot_general | solution.py:44
  25.9 0.7 fusion.12
  26.7 1.6 %convolution_convert_fusion.3 = bf16[16,2048]{1,0:T(8,128)(2,1)S(1)} fusion(bf16[16,256]{1,0:T(8,128)(2,1)S(1)} %reshape.208, bf16[256,2048]{1,0:T(8,128)(2,1)} %param.30), kind=kOutput, calls=%fused_computation.5 | convolution fusion | flops 16809984 | bytes 1122304 | tf_op jit(solution)/shard_map/dot_general | solution.py:107
  28.3 6.2 %all-gather = bf16[64,2048]{1,0:T(8,128)(2,1)S(1)} all-gather(bf16[16,2048]{1,0:T(8,128)(2,1)S(1)} %convolution_convert_fusion.3), channel_id=2, replica_groups=mesh['ep'=8,'tp'=4] {'tp'}, dimensions={0}, use_global_device_ids=true | all-gather | bytes 327680 | tf_op jit(solution)/shard_map/all_gather | solution.py:12
  35.2 1.0 fusion.31
  36.2 0.8 copy.47
  37.6 0.7 multiply_add_fusion
  38.6 15.2 %all_to_all.10 = bf16[8,8,2048]{2,1,0:T(8,128)(2,1)S(1)} all-to-all(bf16[8,8,2048]{2,1,0:T(8,128)(2,1)S(1)} %fusion.1), channel_id=1, replica_groups=mesh['ep'=8,'tp'=4] {'ep'}, dimensions={0} | all-to-all | bytes 524288 | tf_op jit(solution)/shard_map/all_to_all | solution.py:124
  53.8 1.5 %fusion.24 = f32[64,256]{1,0:T(8,128)S(1)} fusion(bf16[1,2048,256]{2,1,0:T(8,128)(2,1)} %param.34, bf16[8,8,2048]{2,1,0:T(8,128)(2,1)S(1)} %all_to_all.10), kind=kOutput, calls=%fused_computation.37 | convolution fusion | flops 67108864 | bytes 1376256 | tf_op jit(solution)/shard_map/dot_general | solution.py:126
  55.3 2.7 %convolution_convert_fusion = bf16[64,2048]{1,0:T(8,128)(2,1)} fusion(bf16[1,256,2048]{2,1,0:T(8,128)(2,1)S(1)} %copy-done, bf16[1,2048,256]{2,1,0:T(8,128)(2,1)} %param.35, bf16[8,8,2048]{2,1,0:T(8,128)(2,1)S(1)} %all_to_all.10, f32[64,256]{1,0:T(8,128)S(1)} %fusion.24), kind=kOutput, calls=%fused_computation.1 | convolution fusion | flops 134447104 | bytes 2686976 | tf_op jit(solution)/shard_map/dot_general | solution.py:129
  58.1 1.5 %fusion.72 = f32[16,256]{1,0:T(8,128)S(1)} fusion(bf16[2048,256]{1,0:T(8,128)(2,1)} %param.39, bf16[16,2048]{1,0:T(8,128)(2,1)S(1)} %get-tuple-element.6, f32[2048]{0:T(1024)S(1)} %convert_element_type.118, f32[16]{0:T(128)S(1)} %add_rsqrt_fusion), kind=kOutput, calls=%fused_computation.102 | convolution fusion | flops 16908288 | bytes 1138752 | tf_op jit(solution)/shard_map/dot_general | solution.py:138
  59.6 1.4 %convolution_convert_fusion.2 = bf16[16,2048]{1,0:T(8,128)(2,1)} fusion(bf16[256,2048]{1,0:T(8,128)(2,1)S(1)} %copy-done.2, bf16[2048,256]{1,0:T(8,128)(2,1)S(1)} %copy-done.3, f32[16,256]{1,0:T(8,128)S(1)} %fusion.72, bf16[16,2048]{1,0:T(8,128)(2,1)S(1)} %get-tuple-element.6, f32[2048]{0:T(1024)S(1)} %convert_element_type.118, f32[16]{0:T(128)S(1)} %add_rsqrt_fusion), kind=kOutput, calls=%fused_computation.4 | convolution fusion | flops 33742848 | bytes 2252864 | tf_op jit(solution)/shard_map/dot_general | solution.py:141
  61.1 0.7 multiply_add_fusion.1
  61.7 0.7 reshape.218
  62.6 14.6 %reduce-scatter.3.cloned.1.call-done = bf16[64,512]{1,0:T(8,128)(2,1)} async-done(((bf16[64,2048]{1,0:T(8,128)(2,1)}), bf16[64,512]{1,0:T(8,128)(2,1)}) %reduce-scatter.3.cloned.1.call-update) | async-done | bytes 65552 | tf_op jit(solution)/shard_map/reduce_scatter | solution.py:130
  77.2 5.5 %all-to-all-start.1 = ((bf16[8,8,512]{2,1,0:T(8,128)(2,1)}), bf16[8,8,512]{2,1,0:T(8,128)(2,1)S(1)}, u32[]{:S(2)}, u32[]{:S(2)}) async-start(bf16[8,8,512]{2,1,0:T(8,128)(2,1)} %bitcast.72), calls=%async_computation.2 | async-start | bytes 131072 | tf_op jit(solution)/shard_map/all_to_all | solution.py:132
  82.8 6.8 %all-to-all-done.1 = bf16[8,8,512]{2,1,0:T(8,128)(2,1)S(1)} async-done(((bf16[8,8,512]{2,1,0:T(8,128)(2,1)}), bf16[8,8,512]{2,1,0:T(8,128)(2,1)S(1)}, u32[]{:S(2)}, u32[]{:S(2)}) %all-to-all-start.1) | async-done | bytes 65568 | tf_op jit(solution)/shard_map/all_to_all | solution.py:132
  89.7 0.8 fusion.10
  90.5 8.8 %reduce-scatter.5.cloned.1.call-done = bf16[16,512]{1,0:T(8,128)(2,1)} async-done(((bf16[16,2048]{1,0:T(8,128)(2,1)}), bf16[16,512]{1,0:T(8,128)(2,1)}) %reduce-scatter.5.cloned.1.call-update) | async-done | bytes 16400 | tf_op jit(solution)/shard_map/reduce_scatter | solution.py:142
  99.2 1.4 %add_convert_fusion = bf16[16,512]{1,0:T(8,128)(2,1)} fusion(bf16[16,512]{1,0:T(8,128)(2,1)} %reduce-scatter.5.cloned.1.call-done, f32[16,512]{1,0:T(8,128)S(1)} %fusion.10, f32[16]{0:T(128)S(1)} %fusion.20, bf16[16,2048]{1,0:T(8,128)(2,1)S(1)} %get-tuple-element.6, s32[]{:T(128)S(6)} %select_n.15), kind=kLoop, calls=%fused_computation.70 | loop fusion | flops 49152 | bytes 81988 | tf_op jit(solution)/shard_map/convert_element_type | solution.py:146
  (57 shorter events, 3.9 us)
Async XLA Ops:
  6.5 48.8 %copy-start = (bf16[1,256,2048]{2,1,0:T(8,128)(2,1)S(1)}, bf16[1,256,2048]{2,1,0:T(8,128)(2,1)}, u32[]{:S(2)}) copy-start(bf16[1,256,2048]{2,1,0:T(8,128)(2,1)} %param.36) | copy-start | bytes 3145732
  6.5 70.7 %reduce-scatter.3.cloned.1.call-start = ((), (), s32[]{:S(2)}) async-start(), calls=%async_computation.4 | async-start | bytes 327680 | tf_op jit(solution)/shard_map/reduce_scatter | solution.py:130
  15.5 6.5 %copy-start.10 = (bf16[2048,4]{0,1:T(4,128)(2,1)S(1)}, bf16[2048,4]{0,1:T(4,128)(2,1)}, u32[]{:S(2)}) copy-start(bf16[2048,4]{0,1:T(4,128)(2,1)} %param.28) | copy-start | bytes 49156
  15.6 6.5 %copy-start.11 = (f32[4]{0:T(128)S(1)}, f32[4]{0:T(128)}, u32[]{:S(2)}) copy-start(f32[4]{0:T(128)} %param.29) | copy-start | bytes 52
  15.6 6.8 %copy-start.6 = (s32[16]{0:T(128)S(1)}, s32[16]{0:T(128)}, u32[]{:S(2)}) copy-start(s32[16]{0:T(128)} %param.24) | copy-start | bytes 196
  15.6 6.9 %copy-start.7 = (bf16[2048,64]{0,1:T(8,128)(2,1)S(1)}, bf16[2048,64]{0,1:T(8,128)(2,1)}, u32[]{:S(2)}) copy-start(bf16[2048,64]{0,1:T(8,128)(2,1)} %param.26) | copy-start | bytes 786436
  15.6 9.5 %copy-start.8 = (f32[16,4,1024]{2,1,0:T(4,128)S(1)}, f32[16,4,1024]{2,1,0:T(4,128)}, u32[]{:S(2)}) copy-start(f32[16,4,1024]{2,1,0:T(4,128)} %param.23) | copy-start | bytes 786436
  22.1 3.6 %copy-start.9 = (bf16[2048,64]{0,1:T(8,128)(2,1)S(1)}, bf16[2048,64]{0,1:T(8,128)(2,1)}, u32[]{:S(2)}) copy-start(bf16[2048,64]{0,1:T(8,128)(2,1)} %param.27) | copy-start | bytes 786436
  22.4 3.5 %copy-start.1 = (bf16[16,1024,128]{1,2,0:T(8,128)(2,1)S(1)}, bf16[16,1024,128]{1,2,0:T(8,128)(2,1)}, u32[]{:S(2)}) copy-start(bf16[16,1024,128]{1,2,0:T(8,128)(2,1)} %copy.43) | copy-start | bytes 12582916
  24.9 11.3 %copy-start.4 = (bf16[2048]{0:T(1024)(128)(2,1)S(1)}, bf16[2048]{0:T(1024)(128)(2,1)}, u32[]{:S(2)}) copy-start(bf16[2048]{0:T(1024)(128)(2,1)} %param.32) | copy-start | bytes 12292
  26.7 32.9 %copy-start.2 = (bf16[256,2048]{1,0:T(8,128)(2,1)S(1)}, bf16[256,2048]{1,0:T(8,128)(2,1)}, u32[]{:S(2)}) copy-start(bf16[256,2048]{1,0:T(8,128)(2,1)} %param.41) | copy-start | bytes 3145732
  26.7 32.9 %copy-start.3 = (bf16[2048,256]{1,0:T(8,128)(2,1)S(1)}, bf16[2048,256]{1,0:T(8,128)(2,1)}, u32[]{:S(2)}) copy-start(bf16[2048,256]{1,0:T(8,128)(2,1)} %param.40) | copy-start | bytes 3145732
  37.4 1.0 copy-start.5
  58.0 41.2 %reduce-scatter.5.cloned.1.call-start = ((), (), s32[]{:S(2)}) async-start(), calls=%async_computation.5 | async-start | bytes 81920 | tf_op jit(solution)/shard_map/reduce_scatter | solution.py:142
  77.2 12.4 %all-to-all-start.1 = ((bf16[8,8,512]{2,1,0:T(8,128)(2,1)}), bf16[8,8,512]{2,1,0:T(8,128)(2,1)S(1)}, u32[]{:S(2)}, u32[]{:S(2)}) async-start(bf16[8,8,512]{2,1,0:T(8,128)(2,1)} %bitcast.72), calls=%async_computation.2 | async-start | bytes 131072 | tf_op jit(solution)/shard_map/all_to_all | solution.py:132
Sparse Core Ops, SparseCore 0:
  58.2 19.0 reduce-scatter.2
  79.6 19.5 reduce-scatter.4
